TPU v7x, 32 devices: a whole 2x2x4 slice. The times are simulated.
32 devices in a mesh: grp: 2 (over y), ep: 4 (over z), tp: 4 (over x, core).
Axes of the slice: x: 2, y: 2, z: 4, core: 2. Of those that a mesh axis runs over, the one named last changes fastest.
Arguments:
- queries: bfloat16 [1024, 1024], P(('grp', 'ep'), 'tp'), parts along dimension 0, may hold values from -6 to 6
- keys: bfloat16 [1024, 1024], P(('grp', 'ep'), 'tp'), parts along dimension 0, may hold values from -6 to 6
- values: bfloat16 [1024, 1024], P(('grp', 'ep'), 'tp'), parts along dimension 0, may hold values from -6 to 6
- lambdas: float32 [8], P('tp'), may hold values from 0.3 to 0.8
- head_gain: float32 [128], replicated, may hold values from 0.1 to 1.9
- tokens: bfloat16 [2048, 1536], P(('grp', 'ep')), parts along dimension 0, may hold values from -6 to 6
- route_ids: int32 [2048, 2], P(('grp', 'ep')), parts along dimension 0, may hold values from 0 to 3, all different within a row; in each aligned block of 256 rows (0 to 255, 256 to 511, ...) at most 256 rows name the same one
- route_weights: float32 [2048, 2], P(('grp', 'ep')), parts along dimension 0, may hold values from 0.2 to 1
- moe_gain: float32 [1536], replicated, may hold values from 0.1 to 1.9
- w_gate: bfloat16 [4, 1536, 3072], P('ep', None, 'tp'), may hold values from -0.15625 to 0.15625
- w_up: bfloat16 [4, 1536, 3072], P('ep', None, 'tp'), may hold values from -0.15625 to 0.15625
- w_down: bfloat16 [4, 3072, 1536], P('ep', 'tp'), may hold values from -0.109375 to 0.109375
Outputs:
- heads_out: bfloat16 [1024, 1024], P(('grp', 'ep'), 'tp'), parts along dimension 0
- expert_out: bfloat16 [2048, 1536], P(('grp', 'ep'), 'tp'), parts along dimension 0
There are 2 independent parts, one for each index of `grp`. A program takes and returns all parts, laid end to end along the dimension named above; an argument that names none is the same for every part. Nothing has to cross between parts.
Inputs may be any that keep to these rules, and one draw needn't show every extreme that they name: `route_ids`: each row names 2 different experts. In the 256 rows of one device no expert is named more than 256 times, and in every draw some device names some expert exactly 256 times.
All inputs are finite; a program needn't handle non-finite values.
Results may differ from a plain program's by a relative error of at most 0.015.
Values may be sent and summed in bfloat16 or wider, within the bound.
A program may use at most 64 MiB of HBM per device.

v0:
```python
import jax
import jax.numpy as jnp
from jax import lax
from jax.sharding import PartitionSpec as P


def attend(queries, keys, values, lambdas, head_gain):
    row_count = queries.shape[0]
    head_count = lambdas.shape[0]
    head_dim = queries.shape[1] // (2 * head_count)
    value_dim = values.shape[1] // head_count
    query_parts = queries.reshape(row_count, head_count, 2, head_dim)
    score_scale = head_dim ** (-0.5)
    running = jnp.full((head_count, 2, row_count), -1e30, jnp.float32)
    key_piece = lax.all_gather(keys, "ep", axis=0, tiled=True)
    value_piece = lax.all_gather(values, "ep", axis=0, tiled=True)
    count = key_piece.shape[0]
    key_parts = key_piece.reshape(count, head_count, 2, head_dim)
    value_parts = value_piece.reshape(count, head_count, value_dim)
    scores = (
        jnp.einsum("qhcd,khcd->hcqk", query_parts, key_parts, preferred_element_type=jnp.float32)
        * score_scale
    )
    newest = jnp.maximum(running, jnp.max(scores, axis=-1))
    weights_now = jnp.exp(scores - newest[..., None])
    totals = jnp.sum(weights_now, axis=-1)
    sums = jnp.einsum(
        "hcqk,khe->hcqe",
        weights_now.astype(jnp.bfloat16),
        value_parts,
        preferred_element_type=jnp.float32,
    )
    running, totals, sums = (newest, totals, sums)
    means = sums / totals[..., None]
    mixed = means[:, 0] - lambdas[:, None, None] * means[:, 1]
    scaled = mixed * lax.rsqrt(jnp.mean(mixed * mixed, axis=-1, keepdims=True) + 1e-06) * head_gain
    return (
        jnp.transpose(scaled, (1, 0, 2))
        .reshape(row_count, head_count * value_dim)
        .astype(jnp.bfloat16)
    )


def experts(tokens, route_ids, route_weights, moe_gain, w_gate, w_up, w_down):
    row_count, width = tokens.shape
    top_count = route_ids.shape[1]
    ep_size = lax.axis_size("ep")
    tp_size = lax.axis_size("tp")
    expert_count = w_gate.shape[0] * ep_size
    capacity = 2 * row_count * top_count // expert_count
    token_float = tokens.astype(jnp.float32)
    normed = (
        token_float
        * lax.rsqrt(jnp.mean(token_float * token_float, axis=1, keepdims=True) + 1e-06)
        * moe_gain
    ).astype(jnp.bfloat16)
    flat_ids = route_ids.reshape(-1)
    onehot = (flat_ids[:, None] == jnp.arange(expert_count, dtype=jnp.int32)[None, :]).astype(
        jnp.int32
    )
    earlier = jnp.cumsum(onehot, axis=0) - onehot
    position = jnp.sum(earlier * onehot, axis=1)
    slot_index = flat_ids * capacity + position
    owners = (
        jnp.full((expert_count * capacity,), row_count, jnp.int32)
        .at[slot_index]
        .set(jnp.arange(row_count * top_count, dtype=jnp.int32) // top_count)
    )
    padded = jnp.concatenate([normed, jnp.zeros((1, width), jnp.bfloat16)], axis=0)
    outgoing = padded[owners].reshape(expert_count, capacity, width)
    gate_mat = w_gate[0]
    up_mat = w_up[0]
    down_mat = w_down[0]
    slice_width = width // tp_size
    own_columns = lax.dynamic_slice_in_dim(
        outgoing, lax.axis_index("tp") * slice_width, slice_width, 2
    )
    arrived = lax.all_to_all(own_columns, "ep", split_axis=0, concat_axis=0, tiled=True)
    piece = lax.all_gather(arrived, "tp", axis=2, tiled=True)
    gate = jnp.einsum("scd,df->scf", piece, gate_mat, preferred_element_type=jnp.float32)
    upward = jnp.einsum("scd,df->scf", piece, up_mat, preferred_element_type=jnp.float32)
    hidden = (jax.nn.silu(gate) * upward).astype(jnp.bfloat16)
    flat_hidden = hidden.reshape(-1, hidden.shape[2])
    summed = lax.psum_scatter(
        jnp.einsum("fd,sf->ds", down_mat, flat_hidden, preferred_element_type=jnp.float32).astype(
            jnp.bfloat16
        ),
        "tp",
        scatter_dimension=0,
        tiled=True,
    )
    back = lax.all_to_all(summed, "ep", split_axis=1, concat_axis=1, tiled=True)
    picked = (
        jnp.take(back, slot_index, axis=1).astype(jnp.float32).reshape(-1, row_count, top_count)
    )
    combined = jnp.einsum("drk,rk->rd", picked, route_weights)
    return combined.astype(jnp.bfloat16)


def on_device(
    queries,
    keys,
    values,
    lambdas,
    head_gain,
    tokens,
    route_ids,
    route_weights,
    moe_gain,
    w_gate,
    w_up,
    w_down,
):
    heads_out = attend(queries, keys, values, lambdas, head_gain)
    expert_out = experts(tokens, route_ids, route_weights, moe_gain, w_gate, w_up, w_down)
    return (heads_out, expert_out)


def solution(mesh):
    in_specs = (
        P(("grp", "ep"), "tp"),
        P(("grp", "ep"), "tp"),
        P(("grp", "ep"), "tp"),
        P("tp"),
        P(),
        P(("grp", "ep"), None),
        P(("grp", "ep"), None),
        P(("grp", "ep"), None),
        P(),
        P("ep", None, "tp"),
        P("ep", None, "tp"),
        P("ep", "tp", None),
    )
    out_specs = (P(("grp", "ep"), "tp"), P(("grp", "ep"), "tp"))
    return jax.shard_map(
        on_device, mesh=mesh, in_specs=in_specs, out_specs=out_specs, check_vma=False
    )
```

profile of v0, /device:TPU:0, one launch (start us, length us, event | category | flops | bytes accessed | tf_op | source)
XLA Modules:
  0.0 183.2 jit_solution(15858981580019613275)
XLA Ops:
  7.2 1.0 copy.40
  9.2 1.2 reduce-window.6
  11.2 2.4 %scatter_custom_fusion = s32[1024]{0:T(1024)S(1)} fusion(s32[512]{0:T(512)S(1)} %bitcast.95, s32[512]{0:T(512)S(1)} %add_select_fusion, s32[]{:T(128)} %constant.33.clone.1), kind=kCustom, calls=%fused_computation.53 | custom fusion | bytes 4100 | tf_op jit(solution)/shard_map/scatter | solution.py:67
  13.7 1.4 fusion.8
  15.1 1.4 fusion.10
  16.5 5.6 %gather_fusion = bf16[1024,1536]{1,0:T(8,128)(2,1)} fusion(bf16[257,1536]{1,0:T(8,128)(2,1)S(1)} %concatenate.3, s32[1024]{0:T(1024)S(1)} %fusion.23), kind=kCustom, calls=%fused_computation | custom fusion | bytes 6295552 | tf_op jit(solution)/shard_map/gather | solution.py:70
  22.1 1.2 constant_dynamic-slice_fusion
  23.3 26.4 %all_to_all.17 = bf16[4,256,384]{2,1,0:T(8,128)(2,1)} all-to-all(bf16[4,256,384]{2,1,0:T(8,128)(2,1)S(1)} %constant_dynamic-slice_fusion), channel_id=1, replica_groups=mesh['grp'=2,'ep'=4,'tp'=4] {'ep'}, dimensions={0} | all-to-all | bytes 1572864 | tf_op jit(solution)/shard_map/all_to_all | solution.py:78
  49.8 27.7 %all-gather.2.cloned.1.call-done = bf16[4,256,1536]{2,1,0:T(8,128)(2,1)} async-done(((bf16[4,256,384]{2,1,0:T(8,128)(2,1)}), bf16[4,256,1536]{2,1,0:T(8,128)(2,1)}) %all-gather.2.cloned.1.call-update) | async-done | bytes 3145744 | tf_op jit(solution)/shard_map/all_gather | solution.py:79
  77.5 5.4 %fusion.2 = f32[4,256,768]{2,1,0:T(8,128)S(1)} fusion(bf16[4,256,1536]{2,1,0:T(8,128)(2,1)} %all-gather.2.cloned.1.call-done, bf16[1,1536,768]{2,1,0:T(8,128)(2,1)} %param.22), kind=kOutput, calls=%fused_computation.7 | convolution fusion | flops 2415919104 | bytes 8650752 | tf_op jit(solution)/shard_map/scd,df->scf/dot_general | solution.py:81
  82.8 2.9 %multiply_convert_fusion = bf16[4,256,768]{2,1,0:T(8,128)(2,1)S(1)} fusion(f32[4,256,768]{2,1,0:T(8,128)S(1)} %fusion.2, bf16[4,256,1536]{2,1,0:T(8,128)(2,1)S(1)} %copy-done.8, bf16[1,1536,768]{2,1,0:T(8,128)(2,1)S(1)} %copy-done.9), kind=kOutput, calls=%fused_computation.5 | convolution fusion | flops 2420637696 | bytes 10223616 | tf_op jit(solution)/shard_map/scd,df->scf/dot_general | solution.py:80
  85.8 4.0 %fusion = bf16[1536,1024]{0,1:T(8,128)(2,1)} fusion(bf16[1024,768]{1,0:T(8,128)(2,1)S(1)} %bitcast.99, bf16[1,768,1536]{2,1,0:T(8,128)(2,1)S(1)} %copy-done), kind=kOutput, calls=%fused_computation.4 | convolution fusion | flops 2417491968 | bytes 7077888 | tf_op jit(solution)/shard_map/fd,sf->ds/dot_general | solution.py:85
  89.8 4.6 %copy.49 = bf16[1536,1024]{1,0:T(8,128)(2,1)} copy(bf16[1536,1024]{0,1:T(8,128)(2,1)} %fusion) | data formatting | bytes 6291456
  96.7 13.9 %all_gather.9 = bf16[512,256]{1,0:T(8,128)(2,1)S(1)} all-gather(bf16[128,256]{1,0:T(8,128)(2,1)S(1)} %copy-done.1), channel_id=1, replica_groups=mesh['grp'=2,'ep'=4,'tp'=4] {'ep'}, dimensions={0}, use_global_device_ids=true | all-gather | bytes 327680 | tf_op jit(solution)/shard_map/all_gather | solution.py:15
  110.9 1.3 fusion.30
  112.2 20.3 %reduce-scatter.4.cloned.1.call-done = bf16[384,1024]{1,0:T(8,128)(2,1)} async-done(((bf16[1536,1024]{1,0:T(8,128)(2,1)}), bf16[384,1024]{1,0:T(8,128)(2,1)}) %reduce-scatter.4.cloned.1.call-update) | async-done | bytes 786448
  132.5 2.3 %copy.50 = bf16[384,1024]{0,1:T(8,128)(2,1)} copy(bf16[384,1024]{1,0:T(8,128)(2,1)} %reduce-scatter.4.cloned.1.call-done) | data formatting | bytes 1572864
  134.8 4.7 %all-to-all-start.1 = ((bf16[384,4,256]{0,2,1:T(8,128)(2,1)}), bf16[384,4,256]{0,2,1:T(8,128)(2,1)S(1)}, u32[]{:S(2)}, u32[]{:S(2)}) async-start(bf16[384,4,256]{0,2,1:T(8,128)(2,1)} %bitcast.87), calls=%async_computation.1 | async-start | bytes 1572864 | tf_op jit(solution)/shard_map/all_to_all | solution.py:92
  139.5 27.2 %all_gather.10 = bf16[512,256]{1,0:T(8,128)(2,1)S(1)} all-gather(bf16[128,256]{1,0:T(8,128)(2,1)S(1)} %copy-done.2), channel_id=1, replica_groups=mesh['grp'=2,'ep'=4,'tp'=4] {'ep'}, dimensions={0}, use_global_device_ids=true | all-gather | bytes 327680 | tf_op jit(solution)/shard_map/all_gather | solution.py:16
  166.7 0.9 copy.38
  167.6 1.5 fusion.11
  169.1 1.7 convolution_divide_fusion
  171.8 1.9 %gather_fusion.1 = bf16[512,384]{1,0:T(8,128)(2,1)S(1)} fusion(bf16[384,1024]{0,1:T(8,128)(2,1)S(1)} %bitcast.85, s32[1024]{0:T(1024)S(1)} %pad_clamp_fusion), kind=kCustom, calls=%fused_computation.1 | custom fusion | bytes 788480 | tf_op jit(solution)/shard_map/jit(_take)/gather | solution.py:94
  173.9 1.7 fusion.15
  (55 shorter events, 6.3 us)
Async XLA Ops:
  7.2 78.6 %copy-start = (bf16[1,768,1536]{2,1,0:T(8,128)(2,1)S(1)}, bf16[1,768,1536]{2,1,0:T(8,128)(2,1)}, u32[]{:S(2)}) copy-start(bf16[1,768,1536]{2,1,0:T(8,128)(2,1)} %param.23) | copy-start | bytes 7077892
  7.2 70.3 %all-gather.2.cloned.1.call-start = ((), (), s32[]{:S(2)}) async-start(), calls=%async_computation.3 | async-start | bytes 3932160 | tf_op jit(solution)/shard_map/all_gather | solution.py:79
  49.7 82.8 %reduce-scatter.4.cloned.1.call-start = ((), (), s32[]{:S(2)}) async-start(), calls=%async_computation.4 | async-start | bytes 3932160
  77.4 5.4 %copy-start.8 = (bf16[4,256,1536]{2,1,0:T(8,128)(2,1)S(1)}, bf16[4,256,1536]{2,1,0:T(8,128)(2,1)}, u32[]{:S(2)}) copy-start(bf16[4,256,1536]{2,1,0:T(8,128)(2,1)} %all-gather.2.cloned.1.call-done) | copy-start | bytes 9437188
  77.4 5.4 %copy-start.9 = (bf16[1,1536,768]{2,1,0:T(8,128)(2,1)S(1)}, bf16[1,1536,768]{2,1,0:T(8,128)(2,1)}, u32[]{:S(2)}) copy-start(bf16[1,1536,768]{2,1,0:T(8,128)(2,1)} %param.21) | copy-start | bytes 7077892
  94.4 0.7 copy-start.4
  94.4 1.4 copy-start.5
  94.4 2.3 %copy-start.1 = (bf16[128,256]{1,0:T(8,128)(2,1)S(1)}, bf16[128,256]{1,0:T(8,128)(2,1)}, u32[]{:S(2)}) copy-start(bf16[128,256]{1,0:T(8,128)(2,1)} %param.13) | copy-start | bytes 196612
  94.4 16.4 %copy-start.3 = (bf16[128,256]{1,0:T(8,128)(2,1)S(1)}, bf16[128,256]{1,0:T(8,128)(2,1)}, u32[]{:S(2)}) copy-start(bf16[128,256]{1,0:T(8,128)(2,1)} %param.12) | copy-start | bytes 196612
  94.5 45.1 %copy-start.2 = (bf16[128,256]{1,0:T(8,128)(2,1)S(1)}, bf16[128,256]{1,0:T(8,128)(2,1)}, u32[]{:S(2)}) copy-start(bf16[128,256]{1,0:T(8,128)(2,1)} %param.14) | copy-start | bytes 196612
  112.2 58.6 %copy-start.6 = (f32[2]{0:T(128)S(1)}, f32[2]{0:T(128)}, u32[]{:S(2)}) copy-start(f32[2]{0:T(128)} %param.15) | copy-start | bytes 28
  134.8 36.2 %copy-start.7 = (f32[128]{0:T(128)S(1)}, f32[128]{0:T(128)}, u32[]{:S(2)}) copy-start(f32[128]{0:T(128)} %param.16) | copy-start | bytes 1540
  134.8 37.1 %all-to-all-start.1 = ((bf16[384,4,256]{0,2,1:T(8,128)(2,1)}), bf16[384,4,256]{0,2,1:T(8,128)(2,1)S(1)}, u32[]{:S(2)}, u32[]{:S(2)}) async-start(bf16[384,4,256]{0,2,1:T(8,128)(2,1)} %bitcast.87), calls=%async_computation.1 | async-start | bytes 1572864 | tf_op jit(solution)/shard_map/all_to_all | solution.py:92
Sparse Core Ops, SparseCore 0:
  49.8 27.5 all-gather.1
  94.6 37.8 reduce-scatter.3
where the time goes:
time: 184 us; the launch traced here: 183 us
  blocking collectives  67.5 us (37%)
  waiting for transfers between devices  48 us (26%)
  local copies, waits for them, and re-layouts  24.9 us (14%)
  matrix products  17 us (9%)
  between operations  14.3 us (8%)
  other arithmetic  6.72 us (4%)
  starting transfers between devices  4.81 us (3%)
    all_gather x1, waiting for transfers between devices, experts(): piece = lax.all_gather(arrived, 'tp', axis=2, tiled=True)  27.7 us
    all_gather x1, blocking collectives, attend(): value_piece = lax.all_gather(values, 'ep', axis=0, tiled=True)  27.2 us
    all_to_all x1, blocking collectives, experts(): lax.all_to_all(own_columns, 'ep', split_axis=0, concat_axis=0, tiled=True)  26.4 us
    unnamed x3, waiting for transfers between devices  20.3 us
    all_gather x1, blocking collectives, attend(): key_piece = lax.all_gather(keys, 'ep', axis=0, tiled=True)  13.9 us
    unnamed x26, local copies, waits for them, and re-layouts  10 us
    gather x1, local copies, waits for them, and re-layouts, experts(): outgoing = padded[owners].reshape(expert_count, capacity, width)  5.61 us
    dot_general x1, matrix products, experts(): jnp.einsum('scd,df->scf', piece, up_mat, preferred_element_type=jnp.float32)  5.36 us
  transfers between devices with their start and end apart: 3, of which 2 were waited for; matrix products, arithmetic and copies ran while one was open for 5% of the time, Pallas kernels for 0%

commit v1 on v0

--- a/solution.py
+++ b/solution.py
@@ -13,7 +13,12 @@
     score_scale = head_dim ** (-0.5)
     running = jnp.full((head_count, 2, row_count), -1e30, jnp.float32)
     key_piece = lax.all_gather(keys, "ep", axis=0, tiled=True)
-    value_piece = lax.all_gather(values, "ep", axis=0, tiled=True)
+    ring = [values]
+    for hop in range(3):
+        ring.append(lax.ppermute(ring[-1], "ep", [(dev, (dev + 1) % 4) for dev in range(4)]))
+    value_piece = jnp.roll(
+        jnp.concatenate(ring[::-1], axis=0), (lax.axis_index("ep") + 1) * ring[0].shape[0], axis=0
+    )
     count = key_piece.shape[0]
     key_parts = key_piece.reshape(count, head_count, 2, head_dim)
     value_parts = value_piece.reshape(count, head_count, value_dim)

time: 184 us -> 171 us (0.929)
  blocking collectives: 67.5 us -> 40.3 us
  waiting for transfers between devices: 48 us -> 59.8 us
  local copies, waits for them, and re-layouts: 24.9 us -> 27.8 us
  starting transfers between devices: 4.81 us -> 6.84 us
    all_gather x1 -> x0, blocking collectives: 27.2 us -> none  [attend(): value_piece = lax.all_gather(values, 'ep', axis=0, tiled=True)]
    all_to_all x1, waiting for transfers between devices: 0.01 us -> 14.2 us  [experts(): back = lax.all_to_all(summed, 'ep', split_axis=1, concat_axis=1, tiled=True)]
    unnamed x3, waiting for transfers between devices: 20.3 us -> 8.66 us
    ppermute x0 -> x3, waiting for transfers between devices: none -> 9.29 us  [attend(): lax.ppermute(ring[-1], 'ep', [(dev, (dev + 1) % 4) for dev in range(4)])]
    ppermute x0 -> x3, starting transfers between devices: none -> 2.18 us  [attend(): lax.ppermute(ring[-1], 'ep', [(dev, (dev + 1) % 4) for dev in range(4)])]
    unnamed x26 -> x37, local copies, waits for them, and re-layouts: 10 us -> 11.3 us
  transfers between devices with their start and end apart: 3 -> 6, of which waited for: 2 -> 5; matrix products, arithmetic and copies ran while one was open for 5% -> 5% of each run, Pallas kernels for 0% -> 0%
where the time goes in v1:
time: 171 us
  waiting for transfers between devices  59.8 us (35%)
  blocking collectives  40.3 us (24%)
  local copies, waits for them, and re-layouts  27.8 us (16%)
  matrix products  16.1 us (9%)
  between operations  14.4 us (8%)
  starting transfers between devices  6.84 us (4%)
  other arithmetic  5.51 us (3%)
    all_gather x1, waiting for transfers between devices, experts(): piece = lax.all_gather(arrived, 'tp', axis=2, tiled=True)  27.7 us
    all_to_all x1, blocking collectives, experts(): lax.all_to_all(own_columns, 'ep', split_axis=0, concat_axis=0, tiled=True)  26.4 us
    all_to_all x1, waiting for transfers between devices, experts(): back = lax.all_to_all(summed, 'ep', split_axis=1, concat_axis=1, tiled=True)  14.2 us
    all_gather x1, blocking collectives, attend(): key_piece = lax.all_gather(keys, 'ep', axis=0, tiled=True)  13.9 us
    unnamed x37, local copies, waits for them, and re-layouts  11.3 us
    ppermute x3, waiting for transfers between devices, attend(): lax.ppermute(ring[-1], 'ep', [(dev, (dev + 1) % 4) for dev in range(4)])  9.29 us
    unnamed x3, waiting for transfers between devices  8.66 us
    gather x1, local copies, waits for them, and re-layouts, experts(): outgoing = padded[owners].reshape(expert_count, capacity, width)  5.61 us
  transfers between devices with their start and end apart: 6, of which 5 were waited for; matrix products, arithmetic and copies ran while one was open for 5% of the time, Pallas kernels for 0%

profile of v1, /device:TPU:0, one launch (start us, length us, event | category | flops | bytes accessed | tf_op | source)
XLA Modules:
  0.0 170.7 jit_solution(6046883404924101542)
XLA Ops:
  9.2 1.2 reduce-window.6
  11.2 2.4 %scatter_custom_fusion = s32[1024]{0:T(1024)S(1)} fusion(s32[512]{0:T(512)S(1)} %bitcast.95, s32[512]{0:T(512)S(1)} %add_select_fusion, s32[]{:T(128)} %constant.90.clone.1), kind=kCustom, calls=%fused_computation.61 | custom fusion | bytes 4100 | tf_op jit(solution)/shard_map/scatter | solution.py:72
  13.7 1.4 fusion.8
  15.1 1.4 fusion.10
  16.5 5.6 %gather_fusion = bf16[1024,1536]{1,0:T(8,128)(2,1)} fusion(bf16[257,1536]{1,0:T(8,128)(2,1)S(1)} %concatenate.10, s32[1024]{0:T(1024)S(1)} %fusion.23), kind=kCustom, calls=%fused_computation | custom fusion | bytes 6295552 | tf_op jit(solution)/shard_map/gather | solution.py:75
  22.1 1.2 constant_dynamic-slice_fusion
  23.3 26.4 %all_to_all.17 = bf16[4,256,384]{2,1,0:T(8,128)(2,1)} all-to-all(bf16[4,256,384]{2,1,0:T(8,128)(2,1)S(1)} %constant_dynamic-slice_fusion), channel_id=1, replica_groups=mesh['grp'=2,'ep'=4,'tp'=4] {'ep'}, dimensions={0} | all-to-all | bytes 1572864 | tf_op jit(solution)/shard_map/all_to_all | solution.py:83
  49.8 27.7 %all-gather.2.cloned.1.call-done = bf16[4,256,1536]{2,1,0:T(8,128)(2,1)} async-done(((bf16[4,256,384]{2,1,0:T(8,128)(2,1)}), bf16[4,256,1536]{2,1,0:T(8,128)(2,1)}) %all-gather.2.cloned.1.call-update) | async-done | bytes 3145744 | tf_op jit(solution)/shard_map/all_gather | solution.py:84
  77.5 5.4 %fusion.2 = f32[4,256,768]{2,1,0:T(8,128)S(1)} fusion(bf16[4,256,1536]{2,1,0:T(8,128)(2,1)} %all-gather.2.cloned.1.call-done, bf16[1,1536,768]{2,1,0:T(8,128)(2,1)} %param.22), kind=kOutput, calls=%fused_computation.7 | convolution fusion | flops 2415919104 | bytes 8650752 | tf_op jit(solution)/shard_map/scd,df->scf/dot_general | solution.py:86
  82.8 2.9 %multiply_convert_fusion = bf16[4,256,768]{2,1,0:T(8,128)(2,1)S(1)} fusion(f32[4,256,768]{2,1,0:T(8,128)S(1)} %fusion.2, bf16[4,256,1536]{2,1,0:T(8,128)(2,1)S(1)} %copy-done.10, bf16[1,1536,768]{2,1,0:T(8,128)(2,1)S(1)} %copy-done.11), kind=kOutput, calls=%fused_computation.5 | convolution fusion | flops 2420637696 | bytes 10223616 | tf_op jit(solution)/shard_map/scd,df->scf/dot_general | solution.py:85
  85.8 4.0 %fusion = bf16[1536,1024]{0,1:T(8,128)(2,1)} fusion(bf16[1024,768]{1,0:T(8,128)(2,1)S(1)} %bitcast.99, bf16[1,768,1536]{2,1,0:T(8,128)(2,1)S(1)} %copy-done), kind=kOutput, calls=%fused_computation.4 | convolution fusion | flops 2417491968 | bytes 7077888 | tf_op jit(solution)/shard_map/fd,sf->ds/dot_general | solution.py:90
  89.8 4.6 %copy.49 = bf16[1536,1024]{1,0:T(8,128)(2,1)} copy(bf16[1536,1024]{0,1:T(8,128)(2,1)} %fusion) | data formatting | bytes 6291456
  95.3 1.5 collective-permute-start
  96.9 13.9 %all_gather.6 = bf16[512,256]{1,0:T(8,128)(2,1)S(1)} all-gather(bf16[128,256]{1,0:T(8,128)(2,1)S(1)} %copy-done.4), channel_id=1, replica_groups=mesh['grp'=2,'ep'=4,'tp'=4] {'ep'}, dimensions={0}, use_global_device_ids=true | all-gather | bytes 327680 | tf_op jit(solution)/shard_map/all_gather | solution.py:15
  114.5 3.2 %collective-permute-done.1 = bf16[128,256]{1,0:T(8,128)(2,1)S(1)} collective-permute-done((bf16[128,256]{1,0:T(8,128)(2,1)S(1)}, bf16[128,256]{1,0:T(8,128)(2,1)S(1)}, u32[]{:S(2)}, u32[]{:S(2)}) %collective-permute-start.1) | collective-permute-done | bytes 65568 | tf_op jit(solution)/shard_map/ppermute | solution.py:18
  117.8 6.1 %collective-permute-done.2 = bf16[128,256]{1,0:T(8,128)(2,1)S(1)} collective-permute-done((bf16[128,256]{1,0:T(8,128)(2,1)S(1)}, bf16[128,256]{1,0:T(8,128)(2,1)S(1)}, u32[]{:S(2)}, u32[]{:S(2)}) %collective-permute-start.2) | collective-permute-done | bytes 65568 | tf_op jit(solution)/shard_map/ppermute | solution.py:18
  123.9 8.6 %reduce-scatter.4.cloned.1.call-done = bf16[384,1024]{1,0:T(8,128)(2,1)} async-done(((bf16[1536,1024]{1,0:T(8,128)(2,1)}), bf16[384,1024]{1,0:T(8,128)(2,1)}) %reduce-scatter.4.cloned.1.call-update) | async-done | bytes 786448
  132.5 2.3 %copy.50 = bf16[384,1024]{0,1:T(8,128)(2,1)} copy(bf16[384,1024]{1,0:T(8,128)(2,1)} %reduce-scatter.4.cloned.1.call-done) | data formatting | bytes 1572864
  134.8 4.6 %all-to-all-start.1 = ((bf16[384,4,256]{0,2,1:T(8,128)(2,1)}), bf16[384,4,256]{0,2,1:T(8,128)(2,1)S(1)}, u32[]{:S(2)}, u32[]{:S(2)}) async-start(bf16[384,4,256]{0,2,1:T(8,128)(2,1)} %bitcast.87), calls=%async_computation.1 | async-start | bytes 1572864 | tf_op jit(solution)/shard_map/all_to_all | solution.py:97
  140.6 1.0 constant_dynamic-slice_fusion.1
  142.5 1.7 %convolution_divide_fusion = f32[2,2,128,128]{2,3,1,0:T(8,128)S(1)} fusion(bf16[512,2,128,1]{0,2,3,1:T(8,128)(2,1)} %bitcast.91, f32[2,2,128,512]{3,2,1,0:T(8,128)} %copy-done.1, f32[2,2,128]{2,1,0:T(2,128)S(1)} %broadcast_maximum_fusion, f32[2,2,128]{2,1,0:T(2,128)S(1)} %fusion.11), kind=kOutput, calls=%fused_computation.17 | convolution fusion | flops 67698688 | bytes 1576960 | tf_op jit(solution)/shard_map/hcqk,khe->hcqe/dot_general | solution.py:32
  145.2 14.2 %all-to-all-done.1 = bf16[384,4,256]{0,2,1:T(8,128)(2,1)S(1)} async-done(((bf16[384,4,256]{0,2,1:T(8,128)(2,1)}), bf16[384,4,256]{0,2,1:T(8,128)(2,1)S(1)}, u32[]{:S(2)}, u32[]{:S(2)}) %all-to-all-start.1) | async-done | bytes 786464 | tf_op jit(solution)/shard_map/all_to_all | solution.py:97
  159.3 1.9 %gather_fusion.1 = bf16[512,384]{1,0:T(8,128)(2,1)S(1)} fusion(bf16[384,1024]{0,1:T(8,128)(2,1)S(1)} %bitcast.85, s32[1024]{0:T(1024)S(1)} %pad_clamp_fusion), kind=kCustom, calls=%fused_computation.1 | custom fusion | bytes 788480 | tf_op jit(solution)/shard_map/jit(_take)/gather | solution.py:99
  161.4 1.7 %fusion.15 = bf16[256,1,384]{2,1,0:T(2,128)(2,1)S(1)} fusion(bf16[256,2,1]{1,2,0:T(2,128)(2,1)} %copy.47, bf16[384,256,2]{0,2,1:T(2,128)(2,1)S(1)} %gather.11, pred[256,2]{1,0:T(8,128)(4,1)} %copy.43), kind=kOutput, calls=%fused_computation.24 | convolution fusion | flops 589824 | bytes 591360 | tf_op jit(solution)/shard_map/drk,rk->rd/dot_general | solution.py:101
  (73 shorter events, 11.5 us)
Async XLA Ops:
  7.2 78.6 %copy-start = (bf16[1,768,1536]{2,1,0:T(8,128)(2,1)S(1)}, bf16[1,768,1536]{2,1,0:T(8,128)(2,1)}, u32[]{:S(2)}) copy-start(bf16[1,768,1536]{2,1,0:T(8,128)(2,1)} %param.23) | copy-start | bytes 7077892
  7.2 70.3 %all-gather.2.cloned.1.call-start = ((), (), s32[]{:S(2)}) async-start(), calls=%async_computation.3 | async-start | bytes 3932160 | tf_op jit(solution)/shard_map/all_gather | solution.py:84
  49.7 82.8 %reduce-scatter.4.cloned.1.call-start = ((), (), s32[]{:S(2)}) async-start(), calls=%async_computation.4 | async-start | bytes 3932160
  77.4 5.4 %copy-start.10 = (bf16[4,256,1536]{2,1,0:T(8,128)(2,1)S(1)}, bf16[4,256,1536]{2,1,0:T(8,128)(2,1)}, u32[]{:S(2)}) copy-start(bf16[4,256,1536]{2,1,0:T(8,128)(2,1)} %all-gather.2.cloned.1.call-done) | copy-start | bytes 9437188
  77.5 5.4 %copy-start.11 = (bf16[1,1536,768]{2,1,0:T(8,128)(2,1)S(1)}, bf16[1,1536,768]{2,1,0:T(8,128)(2,1)}, u32[]{:S(2)}) copy-start(bf16[1,1536,768]{2,1,0:T(8,128)(2,1)} %param.21) | copy-start | bytes 7077892
  94.4 0.8 copy-start.2
  94.4 2.5 %copy-start.4 = (bf16[128,256]{1,0:T(8,128)(2,1)S(1)}, bf16[128,256]{1,0:T(8,128)(2,1)}, u32[]{:S(2)}) copy-start(bf16[128,256]{1,0:T(8,128)(2,1)} %param.13) | copy-start | bytes 196612
  94.4 16.5 %copy-start.5 = (bf16[128,256]{1,0:T(8,128)(2,1)S(1)}, bf16[128,256]{1,0:T(8,128)(2,1)}, u32[]{:S(2)}) copy-start(bf16[128,256]{1,0:T(8,128)(2,1)} %param.12) | copy-start | bytes 196612
  94.4 16.7 %copy-start.6 = (s32[256,2]{0,1:T(2,128)S(1)}, s32[256,2]{0,1:T(2,128)}, u32[]{:S(2)}) copy-start(s32[256,2]{0,1:T(2,128)} %param.18) | copy-start | bytes 6148
  94.4 19.2 %copy-start.7 = (f32[256,2]{0,1:T(2,128)S(1)}, f32[256,2]{0,1:T(2,128)}, u32[]{:S(2)}) copy-start(f32[256,2]{0,1:T(2,128)} %param.19) | copy-start | bytes 6148
  95.3 16.4 %collective-permute-start = (bf16[128,256]{1,0:T(8,128)(2,1)S(1)}, bf16[128,256]{1,0:T(8,128)(2,1)S(1)}, u32[]{:S(2)}, u32[]{:S(2)}) collective-permute-start(bf16[128,256]{1,0:T(8,128)(2,1)S(1)} %copy-done.2), channel_id=1, source_target_pairs={{0,4},{4,8},{8,12},{12,0},{1,5},{5,9},{9,13},{13,1},{2,6},{6,10},{... | collective-permute-start | bytes 196616 | tf_op jit(solution)/shard_map/ppermute | solution.py:18
  111.6 1.0 copy-start.1
  111.6 6.1 %collective-permute-start.1 = (bf16[128,256]{1,0:T(8,128)(2,1)S(1)}, bf16[128,256]{1,0:T(8,128)(2,1)S(1)}, u32[]{:S(2)}, u32[]{:S(2)}) collective-permute-start(bf16[128,256]{1,0:T(8,128)(2,1)S(1)} %collective-permute-done), channel_id=1, source_target_pairs={{0,4},{4,8},{8,12},{12,0},{1,5},{5,9},{9,13},{13,1},{2,6},{6,10},{... | collective-permute-start | bytes 196616 | tf_op jit(solution)/shard_map/ppermute | solution.py:18
  117.7 6.1 %collective-permute-start.2 = (bf16[128,256]{1,0:T(8,128)(2,1)S(1)}, bf16[128,256]{1,0:T(8,128)(2,1)S(1)}, u32[]{:S(2)}, u32[]{:S(2)}) collective-permute-start(bf16[128,256]{1,0:T(8,128)(2,1)S(1)} %collective-permute-done.1), channel_id=1, source_target_pairs={{0,4},{4,8},{8,12},{12,0},{1,5},{5,9},{9,13},{13,1},{2,6},{6,10},{... | collective-permute-start | bytes 196616 | tf_op jit(solution)/shard_map/ppermute | solution.py:18
  123.9 10.9 %copy-start.3 = (bf16[1024,256]{1,0:T(8,128)(2,1)}, bf16[1024,256]{1,0:T(8,128)(2,1)S(1)}, u32[]{:S(2)}) copy-start(bf16[1024,256]{1,0:T(8,128)(2,1)S(1)} %constant_dynamic-update-slice_fusion.2) | copy-start | bytes 1572868
  123.9 20.3 %copy-start.8 = (f32[2]{0:T(128)S(1)}, f32[2]{0:T(128)}, u32[]{:S(2)}) copy-start(f32[2]{0:T(128)} %param.15) | copy-start | bytes 28
  123.9 20.4 %copy-start.9 = (f32[128]{0:T(128)S(1)}, f32[128]{0:T(128)}, u32[]{:S(2)}) copy-start(f32[128]{0:T(128)} %param.16) | copy-start | bytes 1540
  134.8 24.5 %all-to-all-start.1 = ((bf16[384,4,256]{0,2,1:T(8,128)(2,1)}), bf16[384,4,256]{0,2,1:T(8,128)(2,1)S(1)}, u32[]{:S(2)}, u32[]{:S(2)}) async-start(bf16[384,4,256]{0,2,1:T(8,128)(2,1)} %bitcast.87), calls=%async_computation.1 | async-start | bytes 1572864 | tf_op jit(solution)/shard_map/all_to_all | solution.py:97
Sparse Core Ops, SparseCore 0:
  49.8 27.5 all-gather.1
  94.6 37.9 reduce-scatter.3
